TPU v7x, 32 devices: a whole 2x2x4 slice. The times are simulated.
32 devices in a mesh: sp: 8 (over z, x), tp: 4 (over y, core).
Axes of the slice: x: 2, y: 2, z: 4, core: 2. Of those that a mesh axis runs over, the one named last changes fastest.
Arguments:
- resid: bfloat16 [2048, 4096], P('sp'), may hold values from -6 to 6
- pool_in: bfloat16 [2048, 1024], P('sp', 'tp'), may hold values from -6 to 6
- pool_mix: bfloat16 [4, 256, 256], P('tp'), may hold values from -0.375 to 0.375
- pool_gain: float32 [1024], P('tp'), may hold values from 0.1 to 1.9
- out_proj: bfloat16 [1024, 4096], P('tp'), may hold values from -0.1875 to 0.1875
- norm_gain: float32 [4096], replicated, may hold values from 0.1 to 1.9
- w_gate: bfloat16 [8, 4096, 1024], P('sp', None, 'tp'), may hold values from -0.09375 to 0.09375
- w_up: bfloat16 [8, 4096, 1024], P('sp', None, 'tp'), may hold values from -0.09375 to 0.09375
- w_down: bfloat16 [8, 1024, 4096], P('sp', 'tp'), may hold values from -0.1875 to 0.1875
- routes: int32 [2048, 2], P('sp'), may hold values from 0 to 7, all different within a row; in each aligned block of 64 rows (0 to 63, 64 to 127, ...) at most 32 rows name the same one
- route_weight: float32 [2048, 2], P('sp'), may hold values from 0.25 to 2.5
Outputs:
- layer_out: bfloat16 [2048, 4096], P(('sp', 'tp'))
Inputs may be any that keep to these rules, and one draw needn't show every extreme that they name: `routes`: in each aligned block of 64 tokens no expert is named by more than 32 of the block's rows, and the two experts of a token differ.
All inputs are finite; a program needn't handle non-finite values.
Results may differ from a plain program's by a relative error of at most 0.015.
Values may be sent and summed in bfloat16 or wider, within the bound.
A program may use at most 128 MiB of HBM per device.

v0:
```python
import jax
import jax.numpy as jnp
from jax import lax
from jax.sharding import PartitionSpec as P

GROUPS = 4
EPS = 1e-06


def shifted(x, axis, by):
    count = lax.axis_size(axis)
    pairs = [(i, i + by) for i in range(count) if 0 <= i + by < count]
    return lax.ppermute(x, axis, pairs)


def rounded(value):
    return lax.optimization_barrier(value.astype(jnp.bfloat16)).astype(jnp.float32)


def group_diff(pool_in):
    row_count = pool_in.shape[0]
    reach = 2**GROUPS
    before = shifted(pool_in[row_count - reach :], "sp", 1)
    joined = jnp.concatenate([before, pool_in], axis=0).astype(jnp.float32)
    running = jnp.cumsum(joined, axis=0)
    width = jnp.left_shift(jnp.int32(2), lax.axis_index("tp"))
    lagged = lax.dynamic_slice_in_dim(running, reach - width, row_count, 0)
    total = running[reach:] - lagged
    place = lax.axis_index("sp") * row_count + jnp.arange(row_count, dtype=jnp.int32) + 1
    counted = jnp.minimum(place, width).astype(jnp.float32)
    return (total / counted[:, None] - joined[reach:]).astype(jnp.bfloat16)


def normalize(mixed, norm_gain):
    scale = lax.rsqrt(jnp.mean(mixed * mixed, axis=1, keepdims=True) + EPS)
    return (mixed * scale * norm_gain).astype(jnp.bfloat16)


def slot_plan(route_rows, blocks, capacity, experts):
    row_count, choose = route_rows.shape
    flat_routes = route_rows.reshape(blocks, row_count // blocks * choose)
    onehot = (
        flat_routes[:, :, None] == jnp.arange(experts, dtype=jnp.int32)[None, None, :]
    ).astype(jnp.int32)
    earlier = jnp.cumsum(onehot, axis=1) - onehot
    position = jnp.sum(earlier * onehot, axis=2)
    block_ids = jnp.arange(blocks, dtype=jnp.int32)[:, None]
    return (flat_routes * (blocks * capacity) + block_ids * capacity + position).reshape(-1)


def fill_slots(normed, targets, slot_count):
    row_count, width = normed.shape
    choose = targets.shape[0] // row_count
    sources = jnp.arange(row_count * choose, dtype=jnp.int32) // choose
    owner = jnp.full((slot_count,), row_count, jnp.int32).at[targets].set(sources)
    extended = jnp.concatenate([normed, jnp.zeros((1, width), normed.dtype)], axis=0)
    return extended[owner]


def collect(returned, targets, weights):
    row_count, choose = weights.shape
    picked = returned[targets]
    weighted = picked * weights.reshape(-1, 1)
    return jnp.sum(weighted.reshape(row_count, choose, -1), axis=1)


def expert_part(inputs, w_gate, w_up, w_down):
    gate = jnp.dot(inputs, w_gate[0], preferred_element_type=jnp.float32)
    upper = jnp.dot(inputs, w_up[0], preferred_element_type=jnp.float32)
    hidden = (jax.nn.silu(gate) * upper).astype(jnp.bfloat16)
    return jnp.dot(hidden, w_down[0], preferred_element_type=jnp.float32).astype(jnp.bfloat16)


def on_device(
    resid,
    pool_in,
    pool_mix,
    pool_gain,
    out_proj,
    norm_gain,
    w_gate,
    w_up,
    w_down,
    routes,
    route_weight,
):
    token_count, width = resid.shape
    choose = routes.shape[1]
    experts = lax.axis_size("sp")
    slices = lax.axis_size("tp")
    sub_count = token_count // slices
    capacity = max(2, 2 * sub_count * choose // experts)
    tp_index = lax.axis_index("tp")
    diff = group_diff(pool_in)
    pooled = (jnp.dot(diff, pool_mix[0], preferred_element_type=jnp.float32) * pool_gain).astype(
        jnp.bfloat16
    )
    proj = rounded(
        lax.psum_scatter(
            rounded(jnp.dot(pooled, out_proj, preferred_element_type=jnp.float32)).astype(
                jnp.bfloat16
            ),
            "tp",
            scatter_dimension=0,
            tiled=True,
        ).astype(jnp.float32)
    )
    first = tp_index * sub_count
    mixed = lax.dynamic_slice_in_dim(resid, first, sub_count, 0).astype(jnp.float32) + proj
    normed = normalize(mixed, norm_gain)
    route_rows = lax.dynamic_slice_in_dim(routes, first, sub_count, 0)
    weight_rows = lax.dynamic_slice_in_dim(route_weight, first, sub_count, 0)
    targets = slot_plan(route_rows, 1, capacity, experts)
    outgoing = fill_slots(normed, targets, experts * capacity).reshape(experts, capacity, width)
    arrived = lax.all_to_all(outgoing, "sp", split_axis=0, concat_axis=0, tiled=True)
    block_rows = lax.all_gather(arrived, "tp", axis=0, tiled=True)
    spread = expert_part(block_rows.reshape(-1, width), w_gate, w_up, w_down).reshape(
        block_rows.shape
    )
    stacked = spread.reshape((slices,) + arrived.shape)
    received = lax.all_to_all(stacked, "tp", split_axis=0, concat_axis=0, tiled=True)
    summed = jnp.sum(received.astype(jnp.float32), axis=0)
    returned = lax.all_to_all(
        summed.astype(jnp.bfloat16), "sp", split_axis=0, concat_axis=0, tiled=True
    ).astype(summed.dtype)
    moe = collect(returned.reshape(-1, width), targets, weight_rows)
    return (mixed + moe).astype(jnp.bfloat16)


def solution(mesh):
    in_specs = (
        P("sp", None),
        P("sp", "tp"),
        P("tp", None, None),
        P("tp"),
        P("tp", None),
        P(),
        P("sp", None, "tp"),
        P("sp", None, "tp"),
        P("sp", "tp", None),
        P("sp", None),
        P("sp", None),
    )
    out_specs = P(("sp", "tp"), None)
    return jax.shard_map(
        on_device, mesh=mesh, in_specs=in_specs, out_specs=out_specs, check_vma=False
    )
```

profile of v0, /device:TPU:0, one launch (start us, length us, event | category | flops | bytes accessed | tf_op | source)
XLA Modules:
  0.0 365.1 jit_solution(666184547438477695)
XLA Ops:
  6.5 0.0 reduce-scatter.2.cloned.1.call-start
  6.5 0.8 slice.19
  7.4 4.9 %collective-permute-start = (bf16[16,256]{1,0:T(8,128)(2,1)S(1)}, bf16[16,256]{1,0:T(8,128)(2,1)S(1)}, u32[]{:S(2)}, u32[]{:S(2)}) collective-permute-start(bf16[16,256]{1,0:T(8,128)(2,1)S(1)} %slice.19), channel_id=1, source_target_pairs={{0,4},{4,8},{8,12},{12,16},{16,20},{20,24},{24,28},{1,5},{5,9},{9,... | collective-permute-start | bytes 24584 | tf_op jit(solution)/shard_map/ppermute | solution.py:13
  12.3 1.3 collective-permute-done
  13.6 0.9 fusion.24
  14.5 0.0 copy-start.2
  14.6 0.0 copy-start.4
  14.6 0.3 fusion.12
  14.9 0.1 broadcast_add_fusion
  15.0 0.1 copy.22
  15.1 0.3 copy-done.2
  15.5 3.8 %convolution_convert_fusion.1 = bf16[256,4096]{1,0:T(8,128)(2,1)} fusion(bf16[256,4096]{1,0:T(8,128)(2,1)} %param.15, f32[272,256]{1,0:T(8,128)S(1)} %get-tuple-element.8, f32[384,256]{1,0:T(8,128)S(1)} %bitcast.45, f32[272,256]{1,0:T(8,128)S(1)} %slice.32, s32[]{:T(128)S(6)} %select_n.28, bf16[1,256,256]{2,1,0:T(8,128)(2,1)S(1)} %copy-done.2, ...), kind=kOutput, calls=%fused_computation.4 | convolution fusion | flops 571867136 | bytes 5113860 | tf_op jit(solution)/shard_map/dot_general | solution.py:100
  19.3 0.0 reduce-scatter.2.cloned.1.call-update
  19.3 0.0 all-gather.2.cloned.1.call-start
  19.4 0.6 copy-done.5
  20.0 0.1 broadcast_multiply_fusion
  20.0 0.1 copy.24
  20.1 0.1 eq.27
  20.3 0.1 fusion.23
  20.4 0.2 reduce_window_sum.28
  20.6 0.1 copy.23
  20.7 0.1 mul.82
  20.8 0.2 select_reduce_fusion
  21.0 1.0 scatter_custom_fusion
  22.0 30.7 %reduce-scatter.2.cloned.1.call-done = bf16[64,4096]{1,0:T(8,128)(2,1)} async-done(((bf16[256,4096]{1,0:T(8,128)(2,1)}), bf16[64,4096]{1,0:T(8,128)(2,1)}) %reduce-scatter.2.cloned.1.call-update) | async-done | bytes 524304 | tf_op jit(solution)/shard_map/reduce_scatter | solution.py:99
  52.7 1.5 multiply_reduce_fusion.1
  54.2 1.4 multiply_convert_fusion
  55.6 3.2 gather_fusion
  58.8 53.7 %all_to_all.15 = bf16[8,32,4096]{2,1,0:T(8,128)(2,1)} all-to-all(bf16[8,32,4096]{2,1,0:T(8,128)(2,1)} %bitcast.43), channel_id=1, replica_groups=mesh['sp'=8,'tp'=4] {'sp'}, dimensions={0} | all-to-all | bytes 4194304 | tf_op jit(solution)/shard_map/all_to_all | solution.py:115
  112.5 0.0 all-gather.2.cloned.1.call-update
  112.6 56.5 %all-gather.2.cloned.1.call-done = bf16[32,32,4096]{2,1,0:T(8,128)(2,1)} async-done(((bf16[8,32,4096]{2,1,0:T(8,128)(2,1)}), bf16[32,32,4096]{2,1,0:T(8,128)(2,1)}) %all-gather.2.cloned.1.call-update) | async-done | bytes 8388624 | tf_op jit(solution)/shard_map/all_gather | solution.py:116
  169.1 6.5 %fusion.3 = f32[1024,256]{1,0:T(8,128)S(1)} fusion(bf16[1024,4096]{1,0:T(8,128)(2,1)} %bitcast.48, bf16[1,4096,256]{2,1,0:T(8,128)(2,1)} %param.17), kind=kOutput, calls=%fused_computation.9 | convolution fusion | flops 2147483648 | bytes 11534336 | tf_op jit(solution)/shard_map/dot_general | solution.py:68
  175.5 0.0 copy-done.7
  175.5 0.5 copy-done.8
  176.0 2.4 fusion.8
  178.4 2.4 convolution_convert_fusion
  180.8 96.9 %all_to_all.16 = bf16[4,8,32,4096]{3,2,1,0:T(8,128)(2,1)} all-to-all(bf16[4,8,32,4096]{3,2,1,0:T(8,128)(2,1)S(1)} %bitcast.42), channel_id=1, replica_groups=mesh['sp'=8,'tp'=4] {'tp'}, dimensions={0} | all-to-all | bytes 16777216 | tf_op jit(solution)/shard_map/all_to_all | solution.py:121
  277.6 7.0 %reduce_sum.44 = bf16[8,32,4096]{2,1,0:T(8,128)(2,1)} reduce(bf16[4,8,32,4096]{3,2,1,0:T(8,128)(2,1)} %all_to_all.16, bf16[]{:T(256)} %constant.60.clone.1), dimensions={0}, to_apply=%region_7.8 | reduce | flops 3145728 | bytes 10485762 | tf_op jit(solution)/shard_map/reduce_sum | solution.py:122
  284.6 5.6 %all-to-all-start.2 = ((bf16[8,32,4096]{2,1,0:T(8,128)(2,1)}), bf16[8,32,4096]{2,1,0:T(8,128)(2,1)}, u32[]{:S(2)}, u32[]{:S(2)}) async-start(bf16[8,32,4096]{2,1,0:T(8,128)(2,1)} %reduce_sum.44), calls=%async_computation.3 | async-start | bytes 4194304 | tf_op jit(solution)/shard_map/all_to_all | solution.py:123
  290.2 0.1 constant_dynamic-slice_fusion
  290.3 0.1 copy.25
  290.4 47.8 %all-to-all-done.2 = bf16[8,32,4096]{2,1,0:T(8,128)(2,1)} async-done(((bf16[8,32,4096]{2,1,0:T(8,128)(2,1)}), bf16[8,32,4096]{2,1,0:T(8,128)(2,1)}, u32[]{:S(2)}, u32[]{:S(2)}) %all-to-all-start.2) | async-done | bytes 2097184 | tf_op jit(solution)/shard_map/all_to_all | solution.py:123
  338.2 4.0 %bitcast_convert_fusion = f32[256,4096]{1,0:T(8,128)} fusion(bf16[8,32,4096]{2,1,0:T(8,128)(2,1)} %all-to-all-done.2), kind=kLoop, calls=%fused_computation.5 | loop fusion | flops 1048576 | bytes 6291456 | tf_op jit(solution)/shard_map/reshape | solution.py:126
  342.2 5.6 %gather_fusion.1 = f32[128,4096]{1,0:T(8,128)} fusion(f32[256,4096]{1,0:T(8,128)} %bitcast_convert_fusion, s32[1024]{0:T(1024)S(1)} %pad_clamp_fusion), kind=kCustom, calls=%fused_computation.1 | custom fusion | bytes 4194816 | tf_op jit(solution)/shard_map/gather | solution.py:62
  347.9 3.5 gather.10
  351.4 4.8 %multiply_reduce_fusion = f32[64,4096]{1,0:T(8,128)S(1)} fusion(f32[64,2,4096]{2,1,0:T(2,128)} %gather.10, f32[64,2]{1,0:T(8,128)S(1)} %copy.25), kind=kLoop, calls=%fused_computation.11 | loop fusion | flops 786432 | bytes 3146240 | tf_op jit(solution)/shard_map/reduce_sum | solution.py:64
  356.2 0.0 copy-done.1
  356.2 2.0 add_convert_fusion
  (23 shorter events, 0.2 us)
Async XLA Ops:
  6.5 171.9 %copy-start = (bf16[1,256,4096]{2,1,0:T(8,128)(2,1)S(1)}, bf16[1,256,4096]{2,1,0:T(8,128)(2,1)}, u32[]{:S(2)}) copy-start(bf16[1,256,4096]{2,1,0:T(8,128)(2,1)} %param.19) | copy-start | bytes 6291460
  6.5 46.1 %reduce-scatter.2.cloned.1.call-start = ((), (), s32[]{:S(2)}) async-start(), calls=%async_computation.4 | async-start | bytes 2621440 | tf_op jit(solution)/shard_map/reduce_scatter | solution.py:99
  7.4 6.2 %collective-permute-start = (bf16[16,256]{1,0:T(8,128)(2,1)S(1)}, bf16[16,256]{1,0:T(8,128)(2,1)S(1)}, u32[]{:S(2)}, u32[]{:S(2)}) collective-permute-start(bf16[16,256]{1,0:T(8,128)(2,1)S(1)} %slice.19), channel_id=1, source_target_pairs={{0,4},{4,8},{8,12},{12,16},{16,20},{20,24},{24,28},{1,5},{5,9},{9,... | collective-permute-start | bytes 24584 | tf_op jit(solution)/shard_map/ppermute | solution.py:13
  14.5 0.9 copy-start.2
  14.6 0.9 copy-start.4
  19.3 0.7 copy-start.5
  19.3 34.9 %copy-start.3 = (f32[4096]{0:T(1024)S(1)}, f32[4096]{0:T(1024)}, u32[]{:S(2)}) copy-start(f32[4096]{0:T(1024)} %param.16) | copy-start | bytes 49156
  19.3 149.7 %all-gather.2.cloned.1.call-start = ((), (), s32[]{:S(2)}) async-start(), calls=%async_computation.5 | async-start | bytes 10485760 | tf_op jit(solution)/shard_map/all_gather | solution.py:116
  169.1 6.5 %copy-start.7 = (bf16[32,32,4096]{2,1,0:T(8,128)(2,1)S(1)}, bf16[32,32,4096]{2,1,0:T(8,128)(2,1)}, u32[]{:S(2)}) copy-start(bf16[32,32,4096]{2,1,0:T(8,128)(2,1)} %all-gather.2.cloned.1.call-done) | copy-start | bytes 25165828
  169.1 7.0 %copy-start.8 = (bf16[1,4096,256]{2,1,0:T(8,128)(2,1)S(1)}, bf16[1,4096,256]{2,1,0:T(8,128)(2,1)}, u32[]{:S(2)}) copy-start(bf16[1,4096,256]{2,1,0:T(8,128)(2,1)} %param.18) | copy-start | bytes 6291460
  284.6 5.6 %copy-start.6 = (f32[256,2]{0,1:T(2,128)S(1)}, f32[256,2]{0,1:T(2,128)}, u32[]{:S(2)}) copy-start(f32[256,2]{0,1:T(2,128)} %param.21) | copy-start | bytes 6148
  284.6 53.6 %all-to-all-start.2 = ((bf16[8,32,4096]{2,1,0:T(8,128)(2,1)}), bf16[8,32,4096]{2,1,0:T(8,128)(2,1)}, u32[]{:S(2)}, u32[]{:S(2)}) async-start(bf16[8,32,4096]{2,1,0:T(8,128)(2,1)} %reduce_sum.44), calls=%async_computation.3 | async-start | bytes 4194304 | tf_op jit(solution)/shard_map/all_to_all | solution.py:123
  351.4 4.9 %copy-start.1 = (bf16[64,4096]{1,0:T(8,128)(2,1)S(1)}, bf16[64,4096]{1,0:T(8,128)(2,1)}, u32[]{:S(2)}) copy-start(bf16[64,4096]{1,0:T(8,128)(2,1)} %reduce-scatter.2.cloned.1.call-done) | copy-start | bytes 1572868
Sparse Core Ops, SparseCore 0:
  19.4 33.1 reduce-scatter.1
  112.7 56.3 all-gather.1
where the time goes:
time: 366 us; the launch traced here: 365 us
  blocking collectives  151 us (41%)
  waiting for transfers between devices  136 us (37%)
  other arithmetic  22.6 us (6%)
  local copies, waits for them, and re-layouts  16.4 us (4%)
  matrix products  15 us (4%)
  between operations  13.7 us (4%)
  starting transfers between devices  10.5 us (3%)
    all_to_all x1, blocking collectives, on_device(): lax.all_to_all(stacked, 'tp', split_axis=0, concat_axis=0, tiled=True)  96.9 us
    all_gather x1, waiting for transfers between devices, on_device(): block_rows = lax.all_gather(arrived, 'tp', axis=0, tiled=True)  56.5 us
    all_to_all x1, blocking collectives, on_device(): lax.all_to_all(outgoing, 'sp', split_axis=0, concat_axis=0, tiled=True)  53.7 us
    all_to_all x1, waiting for transfers between devices, on_device(): lax.all_to_all(summed.astype(jnp.bfloat16), 'sp', split_axis=0, concat_ax...  47.8 us
    reduce_scatter x1, waiting for transfers between devices, on_device(): lax.psum_scatter(rounded(jnp.dot(pooled, out_proj, preferred_element_type...  30.7 us
    gather x2, local copies, waits for them, and re-layouts, collect(): picked = returned[targets]  9.13 us
  transfers between devices with their start and end apart: 4, of which 4 were waited for; matrix products, arithmetic and copies ran while one was open for 1% of the time, Pallas kernels for 0%

commit v1 on v0

--- a/solution.py
+++ b/solution.py
@@ -113,7 +113,12 @@
     targets = slot_plan(route_rows, 1, capacity, experts)
     outgoing = fill_slots(normed, targets, experts * capacity).reshape(experts, capacity, width)
     arrived = lax.all_to_all(outgoing, "sp", split_axis=0, concat_axis=0, tiled=True)
-    block_rows = lax.all_gather(arrived, "tp", axis=0, tiled=True)
+    ring = [arrived]
+    for hop in range(3):
+        ring.append(lax.ppermute(ring[-1], "tp", [(dev, (dev + 1) % 4) for dev in range(4)]))
+    block_rows = jnp.roll(
+        jnp.concatenate(ring[::-1], axis=0), (lax.axis_index("tp") + 1) * ring[0].shape[0], axis=0
+    )
     spread = expert_part(block_rows.reshape(-1, width), w_gate, w_up, w_down).reshape(
         block_rows.shape
     )

time: 366 us -> 415 us (1.13)
  local copies, waits for them, and re-layouts: 16.4 us -> 46.5 us
  waiting for transfers between devices: 136 us -> 157 us
    ppermute x0 -> x3, waiting for transfers between devices: none -> 76.8 us  [on_device(): lax.ppermute(ring[-1], 'tp', [(dev, (dev + 1) % 4) for dev in range(4)])]
    all_gather x1 -> x0, waiting for transfers between devices: 56.5 us -> none  [on_device(): block_rows = lax.all_gather(arrived, 'tp', axis=0, tiled=True)]
    unnamed x18 -> x35, local copies, waits for them, and re-layouts: 1.43 us -> 22.2 us
    dynamic_slice x0 -> x1, local copies, waits for them, and re-layouts: none -> 7.86 us  [on_device(): jnp.roll(jnp.concatenate(ring[::-1], axis=0), (lax.axis_index('tp') + 1)...]
  transfers between devices with their start and end apart: 4 -> 6, of which waited for: 4 -> 6; matrix products, arithmetic and copies ran while one was open for 1% -> 1% of each run, Pallas kernels for 0% -> 0%
where the time goes in v1:
time: 415 us; the launch traced here: 414 us
  waiting for transfers between devices  157 us (38%)
  blocking collectives  150 us (36%)
  local copies, waits for them, and re-layouts  46.5 us (11%)
  other arithmetic  22.6 us (5%)
  matrix products  14.4 us (3%)
  between operations  13.7 us (3%)
  starting transfers between devices  9.55 us (2%)
    all_to_all x1, blocking collectives, on_device(): lax.all_to_all(stacked, 'tp', split_axis=0, concat_axis=0, tiled=True)  96.9 us
    ppermute x3, waiting for transfers between devices, on_device(): lax.ppermute(ring[-1], 'tp', [(dev, (dev + 1) % 4) for dev in range(4)])  76.8 us
    all_to_all x1, blocking collectives, on_device(): lax.all_to_all(outgoing, 'sp', split_axis=0, concat_axis=0, tiled=True)  53.6 us
    all_to_all x1, waiting for transfers between devices, on_device(): lax.all_to_all(summed.astype(jnp.bfloat16), 'sp', split_axis=0, concat_ax...  47.7 us
    reduce_scatter x1, waiting for transfers between devices, on_device(): lax.psum_scatter(rounded(jnp.dot(pooled, out_proj, preferred_element_type...  30.7 us
    unnamed x35, local copies, waits for them, and re-layouts  22.2 us
    gather x2, local copies, waits for them, and re-layouts, collect(): picked = returned[targets]  9.13 us
  transfers between devices with their start and end apart: 6, of which 6 were waited for; matrix products, arithmetic and copies ran while one was open for 1% of the time, Pallas kernels for 0%

profile of v1, /device:TPU:0, one launch (start us, length us, event | category | flops | bytes accessed | tf_op | source)
XLA Modules:
  0.0 413.7 jit_solution(7765411479227155898)
XLA Ops:
  6.5 0.8 slice.19
  7.4 4.9 %collective-permute-start = (bf16[16,256]{1,0:T(8,128)(2,1)S(1)}, bf16[16,256]{1,0:T(8,128)(2,1)S(1)}, u32[]{:S(2)}, u32[]{:S(2)}) collective-permute-start(bf16[16,256]{1,0:T(8,128)(2,1)S(1)} %slice.19), channel_id=1, source_target_pairs={{0,4},{4,8},{8,12},{12,16},{16,20},{20,24},{24,28},{1,5},{5,9},{9,... | collective-permute-start | bytes 24584 | tf_op jit(solution)/shard_map/ppermute | solution.py:13
  12.3 1.3 collective-permute-done
  13.6 0.9 fusion.24
  14.6 0.3 fusion.12
  15.1 0.3 copy-done.7
  15.5 3.8 convolution_convert_fusion.1
  19.3 0.6 copy-done.10
  20.0 0.1 copy.19
  20.1 0.1 eq.30
  20.4 0.2 reduce_window_sum.28
  20.7 0.1 mul.85
  20.8 0.2 select_reduce_fusion
  21.0 1.0 scatter_custom_fusion
  22.0 30.7 %reduce-scatter.2.cloned.1.call-done = bf16[64,4096]{1,0:T(8,128)(2,1)} async-done(((bf16[256,4096]{1,0:T(8,128)(2,1)}), bf16[64,4096]{1,0:T(8,128)(2,1)}) %reduce-scatter.2.cloned.1.call-update) | async-done | bytes 524304 | tf_op jit(solution)/shard_map/reduce_scatter | solution.py:99
  52.7 1.5 multiply_reduce_fusion.1
  54.2 1.4 multiply_convert_fusion
  55.6 3.2 gather_fusion
  58.8 53.6 %all_to_all.15 = bf16[8,32,4096]{2,1,0:T(8,128)(2,1)S(1)} all-to-all(bf16[8,32,4096]{2,1,0:T(8,128)(2,1)} %bitcast.45), channel_id=1, replica_groups=mesh['sp'=8,'tp'=4] {'sp'}, dimensions={0} | all-to-all | bytes 4194304 | tf_op jit(solution)/shard_map/all_to_all | solution.py:115
  112.4 1.3 copy-done.1
  113.8 25.5 %collective-permute-done.1 = bf16[8,32,4096]{2,1,0:T(8,128)(2,1)S(1)} collective-permute-done((bf16[8,32,4096]{2,1,0:T(8,128)(2,1)S(1)}, bf16[8,32,4096]{2,1,0:T(8,128)(2,1)S(1)}, u32[]{:S(2)}, u32[]{:S(2)}) %collective-permute-start.1) | collective-permute-done | bytes 2097184 | tf_op jit(solution)/shard_map/ppermute | solution.py:118
  139.2 1.3 copy-done.4
  140.6 25.6 %collective-permute-done.2 = bf16[8,32,4096]{2,1,0:T(8,128)(2,1)} collective-permute-done((bf16[8,32,4096]{2,1,0:T(8,128)(2,1)S(1)}, bf16[8,32,4096]{2,1,0:T(8,128)(2,1)}, u32[]{:S(2)}, u32[]{:S(2)}) %collective-permute-start.2) | collective-permute-done | bytes 2097184 | tf_op jit(solution)/shard_map/ppermute | solution.py:118
  166.1 25.8 %collective-permute-done.3 = bf16[8,32,4096]{2,1,0:T(8,128)(2,1)} collective-permute-done((bf16[8,32,4096]{2,1,0:T(8,128)(2,1)}, bf16[8,32,4096]{2,1,0:T(8,128)(2,1)}, u32[]{:S(2)}, u32[]{:S(2)}) %collective-permute-start.3) | collective-permute-done | bytes 2097184 | tf_op jit(solution)/shard_map/ppermute | solution.py:118
  191.9 3.2 constant_dynamic-update-slice_fusion.7
  195.1 3.3 constant_dynamic-update-slice_fusion.6
  198.3 1.5 constant_dynamic-update-slice_fusion.5
  199.8 0.9 copy-done.2
  200.7 1.5 constant_dynamic-update-slice_fusion.4
  202.1 3.2 constant_dynamic-update-slice_fusion.3
  205.3 3.1 constant_dynamic-update-slice_fusion.2
  208.5 1.5 constant_dynamic-update-slice_fusion.1
  210.0 1.5 constant_dynamic-update-slice_fusion
  211.4 7.9 %constant_dynamic-slice_fusion.1 = bf16[32,32,4096]{2,1,0:T(8,128)(2,1)} fusion(bf16[64,32,4096]{2,1,0:T(8,128)(2,1)} %constant_dynamic-update-slice_fusion, s32[]{:T(128)S(6)} %select_n.46), kind=kLoop, calls=%fused_computation.50 | loop fusion | bytes 16777220 | tf_op jit(solution)/shard_map/jit(_roll_dynamic)/dynamic_slice | solution.py:119
  219.3 5.9 %fusion.3 = f32[1024,256]{1,0:T(8,128)S(1)} fusion(bf16[1024,4096]{1,0:T(8,128)(2,1)} %bitcast.43, bf16[1,4096,256]{2,1,0:T(8,128)(2,1)S(1)} %copy-done.12), kind=kOutput, calls=%fused_computation.9 | convolution fusion | flops 2147483648 | bytes 11534336 | tf_op jit(solution)/shard_map/dot_general | solution.py:68
  225.2 0.5 copy-done.13
  225.6 2.4 fusion.8
  228.0 2.4 convolution_convert_fusion
  230.4 96.9 %all_to_all.16 = bf16[4,8,32,4096]{3,2,1,0:T(8,128)(2,1)} all-to-all(bf16[4,8,32,4096]{3,2,1,0:T(8,128)(2,1)S(1)} %bitcast.42), channel_id=1, replica_groups=mesh['sp'=8,'tp'=4] {'tp'}, dimensions={0} | all-to-all | bytes 16777216 | tf_op jit(solution)/shard_map/all_to_all | solution.py:126
  327.3 7.0 %reduce_sum.44 = bf16[8,32,4096]{2,1,0:T(8,128)(2,1)} reduce(bf16[4,8,32,4096]{3,2,1,0:T(8,128)(2,1)} %all_to_all.16, bf16[]{:T(256)} %constant.80.clone.1), dimensions={0}, to_apply=%region_7.8 | reduce | flops 3145728 | bytes 10485762 | tf_op jit(solution)/shard_map/reduce_sum | solution.py:127
  334.2 4.7 %all-to-all-start.2 = ((bf16[8,32,4096]{2,1,0:T(8,128)(2,1)}), bf16[8,32,4096]{2,1,0:T(8,128)(2,1)}, u32[]{:S(2)}, u32[]{:S(2)}) async-start(bf16[8,32,4096]{2,1,0:T(8,128)(2,1)} %reduce_sum.44), calls=%async_computation.3 | async-start | bytes 4194304 | tf_op jit(solution)/shard_map/all_to_all | solution.py:128
  339.0 0.1 copy.20
  339.1 47.7 %all-to-all-done.2 = bf16[8,32,4096]{2,1,0:T(8,128)(2,1)} async-done(((bf16[8,32,4096]{2,1,0:T(8,128)(2,1)}), bf16[8,32,4096]{2,1,0:T(8,128)(2,1)}, u32[]{:S(2)}, u32[]{:S(2)}) %all-to-all-start.2) | async-done | bytes 2097184 | tf_op jit(solution)/shard_map/all_to_all | solution.py:128
  386.9 4.0 bitcast_convert_fusion
  390.9 5.6 %gather_fusion.1 = f32[128,4096]{1,0:T(8,128)} fusion(f32[256,4096]{1,0:T(8,128)} %bitcast_convert_fusion, s32[1024]{0:T(1024)S(1)} %pad_clamp_fusion), kind=kCustom, calls=%fused_computation.1 | custom fusion | bytes 4194816 | tf_op jit(solution)/shard_map/gather | solution.py:62
  396.5 3.5 gather.10
  400.0 4.8 %multiply_reduce_fusion = f32[64,4096]{1,0:T(8,128)S(1)} fusion(f32[64,2,4096]{2,1,0:T(2,128)} %gather.10, f32[64,2]{1,0:T(8,128)S(1)} %copy.20), kind=kLoop, calls=%fused_computation.11 | loop fusion | flops 786432 | bytes 3146240 | tf_op jit(solution)/shard_map/reduce_sum | solution.py:64
  404.9 2.0 add_convert_fusion
  (45 shorter events, 0.7 us)
Async XLA Ops:
  6.5 221.5 %copy-start = (bf16[1,256,4096]{2,1,0:T(8,128)(2,1)S(1)}, bf16[1,256,4096]{2,1,0:T(8,128)(2,1)}, u32[]{:S(2)}) copy-start(bf16[1,256,4096]{2,1,0:T(8,128)(2,1)} %param.19) | copy-start | bytes 6291460
  6.5 46.1 %reduce-scatter.2.cloned.1.call-start = ((), (), s32[]{:S(2)}) async-start(), calls=%async_computation.4 | async-start | bytes 2621440 | tf_op jit(solution)/shard_map/reduce_scatter | solution.py:99
  7.4 6.2 %collective-permute-start = (bf16[16,256]{1,0:T(8,128)(2,1)S(1)}, bf16[16,256]{1,0:T(8,128)(2,1)S(1)}, u32[]{:S(2)}, u32[]{:S(2)}) collective-permute-start(bf16[16,256]{1,0:T(8,128)(2,1)S(1)} %slice.19), channel_id=1, source_target_pairs={{0,4},{4,8},{8,12},{12,16},{16,20},{20,24},{24,28},{1,5},{5,9},{9,... | collective-permute-start | bytes 24584 | tf_op jit(solution)/shard_map/ppermute | solution.py:13
  14.5 0.9 copy-start.7
  14.6 0.9 copy-start.9
  19.3 0.7 copy-start.10
  19.3 34.9 %copy-start.8 = (f32[4096]{0:T(1024)S(1)}, f32[4096]{0:T(1024)}, u32[]{:S(2)}) copy-start(f32[4096]{0:T(1024)} %param.16) | copy-start | bytes 49156
  112.4 1.3 copy-start.1
  113.8 25.5 %collective-permute-start.1 = (bf16[8,32,4096]{2,1,0:T(8,128)(2,1)S(1)}, bf16[8,32,4096]{2,1,0:T(8,128)(2,1)S(1)}, u32[]{:S(2)}, u32[]{:S(2)}) collective-permute-start(bf16[8,32,4096]{2,1,0:T(8,128)(2,1)S(1)} %all_to_all.15), channel_id=1, source_target_pairs={{0,1},{1,2},{2,3},{3,0},{4,5},{5,6},{6,7},{7,4},{8,9},{9,10},{10,1... | collective-permute-start | bytes 6291464 | tf_op jit(solution)/shard_map/ppermute | solution.py:118
  139.2 1.3 copy-start.4
  140.6 25.6 %collective-permute-start.2 = (bf16[8,32,4096]{2,1,0:T(8,128)(2,1)S(1)}, bf16[8,32,4096]{2,1,0:T(8,128)(2,1)}, u32[]{:S(2)}, u32[]{:S(2)}) collective-permute-start(bf16[8,32,4096]{2,1,0:T(8,128)(2,1)S(1)} %collective-permute-done.1), channel_id=1, source_target_pairs={{0,1},{1,2},{2,3},{3,0},{4,5},{5,6},{6,7},{7,4},{8,9},{9,10},{10,1... | collective-permute-start | bytes 6291464 | tf_op jit(solution)/shard_map/ppermute | solution.py:118
  166.1 25.8 %collective-permute-start.3 = (bf16[8,32,4096]{2,1,0:T(8,128)(2,1)}, bf16[8,32,4096]{2,1,0:T(8,128)(2,1)}, u32[]{:S(2)}, u32[]{:S(2)}) collective-permute-start(bf16[8,32,4096]{2,1,0:T(8,128)(2,1)} %collective-permute-done.2), channel_id=1, source_target_pairs={{0,1},{1,2},{2,3},{3,0},{4,5},{5,6},{6,7},{7,4},{8,9},{9,10},{10,1... | collective-permute-start | bytes 6291464 | tf_op jit(solution)/shard_map/ppermute | solution.py:118
  195.1 3.3 copy-start.5
  198.3 2.3 copy-start.2
  211.4 7.9 %copy-start.12 = (bf16[1,4096,256]{2,1,0:T(8,128)(2,1)S(1)}, bf16[1,4096,256]{2,1,0:T(8,128)(2,1)}, u32[]{:S(2)}) copy-start(bf16[1,4096,256]{2,1,0:T(8,128)(2,1)} %param.17) | copy-start | bytes 6291460
  219.3 5.9 %copy-start.3 = (bf16[32,32,4096]{2,1,0:T(8,128)(2,1)S(1)}, bf16[32,32,4096]{2,1,0:T(8,128)(2,1)}, u32[]{:S(2)}) copy-start(bf16[32,32,4096]{2,1,0:T(8,128)(2,1)} %constant_dynamic-slice_fusion.1) | copy-start | bytes 25165828
  219.3 6.4 %copy-start.13 = (bf16[1,4096,256]{2,1,0:T(8,128)(2,1)S(1)}, bf16[1,4096,256]{2,1,0:T(8,128)(2,1)}, u32[]{:S(2)}) copy-start(bf16[1,4096,256]{2,1,0:T(8,128)(2,1)} %param.18) | copy-start | bytes 6291460
  334.2 4.7 %copy-start.11 = (f32[256,2]{0,1:T(2,128)S(1)}, f32[256,2]{0,1:T(2,128)}, u32[]{:S(2)}) copy-start(f32[256,2]{0,1:T(2,128)} %param.21) | copy-start | bytes 6148
  334.2 52.6 %all-to-all-start.2 = ((bf16[8,32,4096]{2,1,0:T(8,128)(2,1)}), bf16[8,32,4096]{2,1,0:T(8,128)(2,1)}, u32[]{:S(2)}, u32[]{:S(2)}) async-start(bf16[8,32,4096]{2,1,0:T(8,128)(2,1)} %reduce_sum.44), calls=%async_computation.3 | async-start | bytes 4194304 | tf_op jit(solution)/shard_map/all_to_all | solution.py:128
  400.0 4.9 %copy-start.6 = (bf16[64,4096]{1,0:T(8,128)(2,1)S(1)}, bf16[64,4096]{1,0:T(8,128)(2,1)}, u32[]{:S(2)}) copy-start(bf16[64,4096]{1,0:T(8,128)(2,1)} %reduce-scatter.2.cloned.1.call-done) | copy-start | bytes 1572868
Sparse Core Ops, SparseCore 0:
  19.4 33.1 reduce-scatter.1
